TPU v7x, 32 devices: a whole 2x2x4 slice. The times are simulated.
32 devices in a mesh: grp: 2 (over y), fs: 4 (over z), tp: 4 (over x, core).
Axes of the slice: x: 2, y: 2, z: 4, core: 2. Of those that a mesh axis runs over, the one named last changes fastest.
Arguments:
- tokens: bfloat16 [8192, 2048], P(('grp', 'fs'), 'tp'), parts along dimension 0, may hold values from -6 to 6
- norm1_gain: float32 [2048], replicated, may hold values from 0.1 to 1.9
- weight_u: float32 [2048, 1024], P('fs', 'tp'), may hold values from -0.125 to 0.125
- weight_v: float32 [2048, 1024], P('fs', 'tp'), may hold values from -0.125 to 0.125
- scale_u: float32 [1024], P('tp'), may hold values from 0.5 to 2
- scale_v: float32 [1024], P('tp'), may hold values from 0.05 to 4.5
- mix_gain: float32 [1024], P('tp'), may hold values from 0.1 to 1.9
- spatial_weight: float32 [4, 128, 128], replicated, may hold values from -0.5 to 0.5
- spatial_bias: float32 [4, 128], replicated, may hold values from 0.5 to 1.5
- weight_out: float32 [1024, 2048], P('tp', 'fs'), may hold values from -0.1875 to 0.1875
- scale_out: float32 [2048], P('fs'), may hold values from 0.5 to 2
- norm2_gain: float32 [2048], replicated, may hold values from 0.1 to 1.9
- weight_up: float32 [2048, 8192], P('fs', 'tp'), may hold values from -0.125 to 0.125
- scale_up: float32 [8192], P('tp'), may hold values from 0.5 to 2
- weight_down: float32 [8192, 2048], P('tp', 'fs'), may hold values from -0.0625 to 0.0625
- scale_down: float32 [2048], P('fs'), may hold values from 0.5 to 2
Outputs:
- result: bfloat16 [8192, 2048], P(('grp', 'fs'), 'tp'), parts along dimension 0
There are 2 independent parts, one for each index of `grp`. A program takes and returns all parts, laid end to end along the dimension named above; an argument that names none is the same for every part. Nothing has to cross between parts.
All inputs are finite; a program needn't handle non-finite values.
Results may differ from a plain program's by a relative error of at most 0.023.
Values may be sent and summed in bfloat16 or wider, within the bound.
A program may use at most 128 MiB of HBM per device.

v0:
```python
import jax
import jax.numpy as jnp
from jax import lax
from jax.sharding import PartitionSpec as P

GM_W = 1024
GROUPS = 4
BLOCK = 128


def per_device(
    tokens,
    norm1_gain,
    weight_u,
    weight_v,
    scale_u,
    scale_v,
    mix_gain,
    spatial_weight,
    spatial_bias,
    weight_out,
    scale_out,
    norm2_gain,
    weight_up,
    scale_up,
    weight_down,
    scale_down,
):
    feature_count = norm1_gain.shape[0]
    out_scales, down_scales = (
        lax.all_gather(scale_out, "fs", axis=0, tiled=True),
        lax.all_gather(scale_down, "fs", axis=0, tiled=True),
    )
    full_u, full_v = (
        lax.all_gather(weight_u.astype(jnp.bfloat16), "fs", axis=0, tiled=True),
        lax.all_gather(weight_v.astype(jnp.bfloat16), "fs", axis=0, tiled=True),
    )
    widened_in = tokens.astype(jnp.float32)
    squares_in = lax.psum(jnp.sum(widened_in * widened_in, axis=1), "tp")
    inverse_in = lax.rsqrt(squares_in / feature_count + 1e-06)[:, None]
    gain_piece = norm1_gain
    normed_piece = (
        lax.all_gather(tokens, "tp", axis=1, tiled=True).astype(jnp.float32)
        * inverse_in
        * gain_piece
    ).astype(jnp.bfloat16)
    pre_u = jnp.dot(normed_piece, full_u, preferred_element_type=jnp.float32)
    pre_v = jnp.dot(normed_piece, full_v, preferred_element_type=jnp.float32)
    gate_u = jax.nn.gelu(pre_u * scale_u)
    act_v = jax.nn.gelu(pre_v * scale_v)
    local_width = act_v.shape[1]
    row_sums, row_squares = lax.psum((jnp.sum(act_v, axis=1), jnp.sum(act_v * act_v, axis=1)), "tp")
    row_mean = (row_sums / GM_W)[:, None]
    square = (row_squares / GM_W)[:, None]
    v_norm = (
        (act_v - row_mean) * lax.rsqrt(square - row_mean * row_mean + 1e-06) * mix_gain
    ).astype(jnp.bfloat16)
    group_index = lax.axis_index("tp") * local_width // (GM_W // GROUPS)
    lower_mask = jnp.tril(jnp.ones((BLOCK, BLOCK), jnp.float32))
    spatial_mask = (
        lax.dynamic_index_in_dim(spatial_weight, group_index, 0, keepdims=False) * lower_mask
    ).astype(jnp.bfloat16)
    block_bias = lax.dynamic_index_in_dim(spatial_bias, group_index, 0, keepdims=False)
    blocks = v_norm.reshape(-1, BLOCK, local_width)
    mixed_cols = jnp.einsum("ts,nsc->ntc", spatial_mask, blocks, preferred_element_type=jnp.float32)
    mixed_cols = mixed_cols + block_bias[None, :, None]
    gated = (gate_u * mixed_cols.reshape(-1, local_width)).astype(jnp.bfloat16)
    out_rounded = weight_out.astype(jnp.bfloat16)
    full_out = lax.all_gather(out_rounded, "fs", axis=1, tiled=True)
    columns = full_out
    piece_scale = out_scales
    product = lax.dot_general(
        columns, gated, (((0,), (1,)), ((), ())), preferred_element_type=jnp.float32
    )
    mixer_sum = (
        lax.psum_scatter(
            (product * piece_scale[:, None]).astype(jnp.bfloat16),
            "tp",
            scatter_dimension=0,
            tiled=True,
        )
        .astype(jnp.float32)
        .T
    )
    residual = (tokens.astype(jnp.float32) + mixer_sum).astype(jnp.bfloat16)
    full_up = lax.all_gather(weight_up.astype(jnp.bfloat16), "fs", axis=0, tiled=True)
    widened_mid = residual.astype(jnp.float32)
    squares_mid = lax.psum(jnp.sum(widened_mid * widened_mid, axis=1), "tp")
    inverse_mid = lax.rsqrt(squares_mid / feature_count + 1e-06)[:, None]
    gain_piece = norm2_gain
    normed_piece = (
        lax.all_gather(residual, "tp", axis=1, tiled=True).astype(jnp.float32)
        * inverse_mid
        * gain_piece
    ).astype(jnp.bfloat16)
    pre_up = jnp.dot(normed_piece, full_up, preferred_element_type=jnp.float32)
    hidden = jnp.square(jax.nn.relu(pre_up * scale_up)).astype(jnp.bfloat16)
    down_rounded = weight_down.astype(jnp.bfloat16)
    full_down = lax.all_gather(down_rounded, "fs", axis=1, tiled=True)
    columns = full_down
    piece_scale = down_scales
    product = lax.dot_general(
        columns, hidden, (((0,), (1,)), ((), ())), preferred_element_type=jnp.float32
    )
    channel_sum = (
        lax.psum_scatter(
            (product * piece_scale[:, None]).astype(jnp.bfloat16),
            "tp",
            scatter_dimension=0,
            tiled=True,
        )
        .astype(jnp.float32)
        .T
    )
    return (residual.astype(jnp.float32) + channel_sum).astype(jnp.bfloat16)


def solution(mesh):
    placed = (
        P(("grp", "fs"), "tp"),
        P(),
        P("fs", "tp"),
        P("fs", "tp"),
        P("tp"),
        P("tp"),
        P("tp"),
        P(),
        P(),
        P("tp", "fs"),
        P("fs"),
        P(),
        P("fs", "tp"),
        P("tp"),
        P("tp", "fs"),
        P("fs"),
    )
    return jax.shard_map(
        per_device, mesh=mesh, in_specs=placed, out_specs=P(("grp", "fs"), "tp"), check_vma=False
    )
```

profile of v0, /device:TPU:0, one launch (start us, length us, event | category | flops | bytes accessed | tf_op | source)
XLA Modules:
  0.0 601.0 jit_solution(15916655100287442903)
XLA Ops:
  6.5 1.8 convert_element_type.74
  8.4 0.7 all-gather.10.cloned.1.call-update
  9.1 1.8 convert_element_type.73
  10.9 0.0 all-gather.16.cloned.1.call-start
  11.0 1.8 convert_element_type.79
  12.8 1.5 fusion.8
  14.3 8.4 %psum.28 = f32[1024]{0:T(1024)S(1)} all-reduce(f32[1024]{0:T(1024)S(1)} %fusion.8), channel_id=1, replica_groups=mesh['grp'=2,'fs'=4,'tp'=4] {'tp'}, use_global_device_ids=true, to_apply=%region_1.0 | all-reduce | flops 1024 | bytes 8192 | tf_op jit(solution)/shard_map/psum | solution.py:39
  22.7 12.7 %all-gather = f32[4,1,512]{2,1,0:T(1,128)S(1)} all-gather(f32[1,1,512]{2,1,0:T(1,128)} %bitcast.33), channel_id=1, replica_groups=mesh['grp'=2,'fs'=4,'tp'=4] {'fs'}, dimensions={0}, use_global_device_ids=true | all-gather | bytes 10240 | tf_op jit(solution)/shard_map/all_gather | solution.py:31
  35.5 4.3 all-gather.14.cloned.1.call-done
  39.8 35.4 %all-gather.10.cloned.1.call-done = bf16[1024,2048]{1,0:T(8,128)(2,1)} async-done(((bf16[1024,512]{1,0:T(8,128)(2,1)}), bf16[1024,2048]{1,0:T(8,128)(2,1)}) %all-gather.10.cloned.1.call-update) | async-done | bytes 4194320 | tf_op jit(solution)/shard_map/all_gather | solution.py:43
  75.2 4.2 fusion.45
  79.4 6.0 %all-reduce = (f32[1024]{0:T(1024)S(1)}, f32[1024]{0:T(1024)S(1)}) all-reduce(f32[1024]{0:T(1024)S(1)} %get-tuple-element.6, f32[1024]{0:T(1024)S(1)} %get-tuple-element.5), channel_id=1, replica_groups=mesh['grp'=2,'fs'=4,'tp'=4] {'tp'}, use_global_device_ids=true, to_apply=%region_5.0 | all-reduce | flops 2048 | bytes 16384 | tf_op jit(solution)/shard_map/psum | solution.py:52
  85.4 0.3 multiply_convert_fusion.21
  85.8 1.1 convolution_add_fusion
  86.9 17.9 %all-gather.12.cloned.1.call-done = bf16[2048,256]{1,0:T(8,128)(2,1)} async-done(((bf16[512,256]{1,0:T(8,128)(2,1)}), bf16[2048,256]{1,0:T(8,128)(2,1)}) %all-gather.12.cloned.1.call-update) | async-done | bytes 1048592 | tf_op jit(solution)/shard_map/all_gather | solution.py:35
  104.8 28.8 %all-gather.16.cloned.1.call-done = bf16[256,2048]{1,0:T(8,128)(2,1)} async-done(((bf16[256,512]{1,0:T(8,128)(2,1)}), bf16[256,2048]{1,0:T(8,128)(2,1)}) %all-gather.16.cloned.1.call-update) | async-done | bytes 1048592 | tf_op jit(solution)/shard_map/all_gather | solution.py:69
  133.6 9.3 %fusion.6 = bf16[2048,1024]{0,1:T(8,128)(2,1)} fusion(f32[2048]{0:T(1024)S(1)} %bitcast.31, bf16[256,2048]{1,0:T(8,128)(2,1)} %all-gather.16.cloned.1.call-done, f32[1024,256]{1,0:T(8,128)S(1)} %bitcast.30, bf16[2048,256]{1,0:T(8,128)(2,1)} %all-gather.12.cloned.1.call-done, bf16[1024,2048]{1,0:T(8,128)(2,1)} %all-gather.10.cloned.1.call-done, ...), kind=kOutput, calls=%fused_computation.9 | convolution fusion | flops 2162950144 | bytes 11555840 | tf_op jit(solution)/shard_map/dot_general | solution.py:72
  142.9 0.0 all-gather.20.cloned.1.call-start
  143.0 3.9 convert_element_type.86
  146.9 0.0 all-gather.22.cloned.1.call-start
  147.0 4.4 convert_element_type.88
  151.5 35.4 %reduce-scatter.3.cloned.1.call-done = bf16[512,1024]{0,1:T(8,128)(2,1)} async-done(((bf16[2048,1024]{0,1:T(8,128)(2,1)}), bf16[512,1024]{0,1:T(8,128)(2,1)}) %reduce-scatter.3.cloned.1.call-update) | async-done | bytes 1048592 | tf_op jit(solution)/shard_map/reduce_scatter | solution.py:76
  186.8 2.6 fusion.10
  189.5 0.0 reduce-scatter.5.cloned.1.call-start
  189.5 12.0 %all-gather.1 = f32[4,1,512]{2,1,0:T(1,128)S(1)} all-gather(f32[1,1,512]{2,1,0:T(1,128)S(1)} %bitcast.34), channel_id=1, replica_groups=mesh['grp'=2,'fs'=4,'tp'=4] {'fs'}, dimensions={0}, use_global_device_ids=true | all-gather | bytes 10240 | tf_op jit(solution)/shard_map/all_gather | solution.py:32
  201.5 6.0 %psum.31 = f32[1024]{0:T(1024)S(1)} all-reduce(f32[1024]{0:T(1024)S(1)} %get-tuple-element.9), channel_id=1, replica_groups=mesh['grp'=2,'fs'=4,'tp'=4] {'tp'}, use_global_device_ids=true, to_apply=%region_8.9 | all-reduce | flops 1024 | bytes 8192 | tf_op jit(solution)/shard_map/psum | solution.py:88
  207.6 130.4 %all-gather.20.cloned.1.call-done = bf16[2048,2048]{1,0:T(8,128)(2,1)} async-done(((bf16[512,2048]{1,0:T(8,128)(2,1)}), bf16[2048,2048]{1,0:T(8,128)(2,1)}) %all-gather.20.cloned.1.call-update) | async-done | bytes 8388624 | tf_op jit(solution)/shard_map/all_gather | solution.py:86
  337.9 149.4 %all-gather.22.cloned.1.call-done = bf16[2048,2048]{1,0:T(8,128)(2,1)} async-done(((bf16[2048,512]{1,0:T(8,128)(2,1)}), bf16[2048,2048]{1,0:T(8,128)(2,1)}) %all-gather.22.cloned.1.call-update) | async-done | bytes 8388624 | tf_op jit(solution)/shard_map/all_gather | solution.py:99
  487.3 34.2 %all-gather.18.cloned.1.call-done = bf16[1024,2048]{1,0:T(8,128)(2,1)} async-done(((bf16[1024,512]{1,0:T(8,128)(2,1)}), bf16[1024,2048]{1,0:T(8,128)(2,1)}) %all-gather.18.cloned.1.call-update) | async-done | bytes 4194320 | tf_op jit(solution)/shard_map/all_gather | solution.py:92
  521.6 25.7 %fusion.7 = bf16[2048,1024]{0,1:T(8,128)(2,1)} fusion(f32[2048]{0:T(1024)S(1)} %bitcast.32, bf16[2048,2048]{1,0:T(8,128)(2,1)} %all-gather.22.cloned.1.call-done, bf16[2048,2048]{1,0:T(8,128)(2,1)} %all-gather.20.cloned.1.call-done, bf16[1024,2048]{1,0:T(8,128)(2,1)} %all-gather.18.cloned.1.call-done, f32[2048]{0:T(1024)S(1)} %copy-done.6, ...), kind=kOutput, calls=%fused_computation.10 | convolution fusion | flops 17200840704 | bytes 25194496 | tf_op jit(solution)/shard_map/dot_general | solution.py:102
  547.3 44.6 %reduce-scatter.5.cloned.1.call-done = bf16[512,1024]{0,1:T(8,128)(2,1)} async-done(((bf16[2048,1024]{0,1:T(8,128)(2,1)}), bf16[512,1024]{0,1:T(8,128)(2,1)}) %reduce-scatter.5.cloned.1.call-update) | async-done | bytes 1048592 | tf_op jit(solution)/shard_map/reduce_scatter | solution.py:106
  591.9 2.5 fusion.11
  (35 shorter events, 0.4 us)
Async XLA Ops:
  6.5 28.9 %copy-start = (f32[4,128]{1,0:T(4,128)S(1)}, f32[4,128]{1,0:T(4,128)}, u32[]{:S(2)}) copy-start(f32[4,128]{1,0:T(4,128)} %param.24) | copy-start | bytes 6148
  6.5 33.2 %all-gather.14.cloned.1.call-start = ((), (), s32[]{:S(2)}) async-start(), calls=%async_computation.4 | async-start | bytes 1310720 | tf_op jit(solution)/shard_map/all_gather | solution.py:36
  8.3 66.9 %all-gather.10.cloned.1.call-start = ((), (), s32[]{:S(2)}) async-start(), calls=%async_computation.2 | async-start | bytes 5242880 | tf_op jit(solution)/shard_map/all_gather | solution.py:43
  9.1 95.7 %all-gather.12.cloned.1.call-start = ((), (), s32[]{:S(2)}) async-start(), calls=%async_computation.3 | async-start | bytes 1310720 | tf_op jit(solution)/shard_map/all_gather | solution.py:35
  10.9 122.7 %all-gather.16.cloned.1.call-start = ((), (), s32[]{:S(2)}) async-start(), calls=%async_computation.5 | async-start | bytes 1310720 | tf_op jit(solution)/shard_map/all_gather | solution.py:69
  12.8 174.1 %reduce-scatter.3.cloned.1.call-start = ((), (), s32[]{:S(2)}) async-start(), calls=%async_computation.6 | async-start | bytes 5242880 | tf_op jit(solution)/shard_map/reduce_scatter | solution.py:76
  35.4 50.0 %copy-start.4 = (f32[256]{0:T(256)S(1)}, f32[256]{0:T(256)}, u32[]{:S(2)}) copy-start(f32[256]{0:T(256)} %param.22) | copy-start | bytes 3076
  35.4 98.2 %copy-start.5 = (f32[2048]{0:T(1024)S(1)}, f32[2048]{0:T(1024)}, u32[]{:S(2)}) copy-start(f32[2048]{0:T(1024)} %param.17) | copy-start | bytes 24580
  35.4 98.2 %copy-start.8 = (f32[256]{0:T(256)S(1)}, f32[256]{0:T(256)}, u32[]{:S(2)}) copy-start(f32[256]{0:T(256)} %param.20) | copy-start | bytes 3076
  142.9 43.9 %copy-start.2 = (bf16[1024,512]{1,0:T(8,128)(2,1)S(1)}, bf16[1024,512]{1,0:T(8,128)(2,1)}, u32[]{:S(2)}) copy-start(bf16[1024,512]{1,0:T(8,128)(2,1)} %param.16) | copy-start | bytes 3145732
  142.9 195.0 %all-gather.20.cloned.1.call-start = ((), (), s32[]{:S(2)}) async-start(), calls=%async_computation.8 | async-start | bytes 10485760 | tf_op jit(solution)/shard_map/all_gather | solution.py:86
  146.9 42.6 %copy-start.3 = (f32[512]{0:T(512)S(1)}, f32[512]{0:T(512)}, u32[]{:S(2)}) copy-start(f32[512]{0:T(512)} %param.31) | copy-start | bytes 6148
  146.9 374.6 %copy-start.6 = (f32[2048]{0:T(1024)S(1)}, f32[2048]{0:T(1024)}, u32[]{:S(2)}) copy-start(f32[2048]{0:T(1024)} %param.29) | copy-start | bytes 24580
  146.9 374.6 %copy-start.7 = (f32[2048]{0:T(1024)S(1)}, f32[2048]{0:T(1024)}, u32[]{:S(2)}) copy-start(f32[2048]{0:T(1024)} %param.27) | copy-start | bytes 24580
  146.9 340.4 %all-gather.22.cloned.1.call-start = ((), (), s32[]{:S(2)}) async-start(), calls=%async_computation.9 | async-start | bytes 10485760 | tf_op jit(solution)/shard_map/all_gather | solution.py:99
  151.4 370.1 %all-gather.18.cloned.1.call-start = ((), (), s32[]{:S(2)}) async-start(), calls=%async_computation.7 | async-start | bytes 5242880 | tf_op jit(solution)/shard_map/all_gather | solution.py:92
  189.5 402.4 %reduce-scatter.5.cloned.1.call-start = ((), (), s32[]{:S(2)}) async-start(), calls=%async_computation.10 | async-start | bytes 5242880 | tf_op jit(solution)/shard_map/reduce_scatter | solution.py:106
  521.6 70.3 %copy-start.1 = (bf16[1024,512]{1,0:T(8,128)(2,1)S(1)}, bf16[1024,512]{1,0:T(8,128)(2,1)}, u32[]{:S(2)}) copy-start(bf16[1024,512]{1,0:T(8,128)(2,1)} %get-tuple-element.10) | copy-start | bytes 3145732
Sparse Core Ops, SparseCore 0:
  8.9 30.8 all-gather.13
  41.3 33.8 all-gather.9
  76.8 27.9 all-gather.11
  106.2 27.3 all-gather.15
  143.1 43.7 reduce-scatter.2
  188.3 149.6 all-gather.19
  339.5 147.7 all-gather.21
  488.9 32.6 all-gather.17
  547.5 44.3 reduce-scatter.4
where the time goes:
time: 601 us
  waiting for transfers between devices  481 us (80%)
  blocking collectives  45.1 us (8%)
  matrix products  40.3 us (7%)
  other arithmetic  20.6 us (3%)
  between operations  13.3 us (2%)
    all_gather x1, waiting for transfers between devices, per_device(): full_down = lax.all_gather(down_rounded, 'fs', axis=1, tiled=True)  149 us
    all_gather x1, waiting for transfers between devices, per_device(): lax.all_gather(weight_up.astype(jnp.bfloat16), 'fs', axis=0, tiled=True)  130 us
    reduce_scatter x2, waiting for transfers between devices, per_device(): lax.psum_scatter((product * piece_scale[:, None]).astype(jnp.bfloat16), '...  79.9 us
    all_gather x1, waiting for transfers between devices, per_device(): lax.all_gather(tokens, 'tp', axis=1, tiled=True).astype(jnp.float32)  35.4 us
    all_gather x1, waiting for transfers between devices, per_device(): lax.all_gather(residual, 'tp', axis=1, tiled=True).astype(jnp.float32)  34.2 us
    all_gather x1, waiting for transfers between devices, per_device(): full_out = lax.all_gather(out_rounded, 'fs', axis=1, tiled=True)  28.8 us
    dot_general x1, matrix products, per_device(): lax.dot_general(columns, hidden, (((0,), (1,)), ((), ())), preferred_elem...  25.7 us
    all_gather x1, waiting for transfers between devices, per_device(): lax.all_gather(weight_u.astype(jnp.bfloat16), 'fs', axis=0, tiled=True)  17.9 us
  transfers between devices with their start and end apart: 9, of which 9 were waited for; matrix products, arithmetic and copies ran while one was open for 4% of the time, Pallas kernels for 0%

commit v1 on v0

--- a/solution.py
+++ b/solution.py
@@ -6,6 +6,18 @@
 GM_W = 1024
 GROUPS = 4
 BLOCK = 128
+
+
+def create_widths(vals, axis_key, dim_no):
+    n_parts = lax.psum(1, axis_name=axis_key)
+    arrivals = [(i, (i + 1) % n_parts) for i in range(n_parts)]
+    z = [None] * n_parts
+    z[n_parts - 1] = vals
+    for h in range(n_parts - 2, -1, -1):
+        z[h] = lax.ppermute(z[h + 1], perm=arrivals, axis_name=axis_key)
+    ready = jnp.concatenate(z, axis=dim_no)
+    far_arr = (lax.axis_index(axis_key) + 1) * vals.shape[dim_no]
+    return jnp.roll(ready, far_arr, axis=dim_no)
 
 
 def per_device(
@@ -96,7 +108,7 @@
     pre_up = jnp.dot(normed_piece, full_up, preferred_element_type=jnp.float32)
     hidden = jnp.square(jax.nn.relu(pre_up * scale_up)).astype(jnp.bfloat16)
     down_rounded = weight_down.astype(jnp.bfloat16)
-    full_down = lax.all_gather(down_rounded, "fs", axis=1, tiled=True)
+    full_down = create_widths(down_rounded, "fs", 1)
     columns = full_down
     piece_scale = down_scales
     product = lax.dot_general(

time: 601 us -> 540 us (0.90)
  waiting for transfers between devices: 481 us -> 278 us
  blocking collectives: 45.1 us -> 136 us
  starting transfers between devices: 0.33 us -> 36.3 us
  local copies, waits for them, and re-layouts: 0.05 us -> 14.6 us
    all_gather x1 -> x0, waiting for transfers between devices: 149 us -> none  [per_device(): full_down = lax.all_gather(down_rounded, 'fs', axis=1, tiled=True)]
    ppermute x0 -> x3, waiting for transfers between devices: none -> 138 us  [create_widths(): z[h] = lax.ppermute(z[h + 1], perm=arrivals, axis_name=axis_key)]
    all_gather x1, waiting for transfers between devices: 130 us -> 0.01 us  [per_device(): lax.all_gather(weight_up.astype(jnp.bfloat16), 'fs', axis=0, tiled=True)]
    all_gather x1, blocking collectives: 12 us -> 104 us  [per_device(): lax.all_gather(scale_down, 'fs', axis=0, tiled=True)]
    ppermute x0 -> x3, starting transfers between devices: none -> 36 us  [create_widths(): z[h] = lax.ppermute(z[h + 1], perm=arrivals, axis_name=axis_key)]
    reduce_scatter x2, waiting for transfers between devices: 79.9 us -> 44.6 us  [per_device(): lax.psum_scatter((product * piece_scale[:, None]).astype(jnp.bfloat16), '...]
    all_gather x1, waiting for transfers between devices: 34.2 us -> 7.22 us  [per_device(): lax.all_gather(residual, 'tp', axis=1, tiled=True).astype(jnp.float32)]
    unnamed x18 -> x30, local copies, waits for them, and re-layouts: 0.04 us -> 14.6 us
  transfers between devices with their start and end apart: 9 -> 11, of which waited for: 9 -> 8; matrix products, arithmetic and copies ran while one was open for 4% -> 6% of each run, Pallas kernels for 0% -> 0%
where the time goes in v1:
time: 540 us
  waiting for transfers between devices  278 us (51%)
  blocking collectives  136 us (25%)
  matrix products  40.4 us (7%)
  starting transfers between devices  36.3 us (7%)
  other arithmetic  20.1 us (4%)
  local copies, waits for them, and re-layouts  14.6 us (3%)
  between operations  13.7 us (3%)
    ppermute x3, waiting for transfers between devices, create_widths(): z[h] = lax.ppermute(z[h + 1], perm=arrivals, axis_name=axis_key)  138 us
    all_gather x1, blocking collectives, per_device(): lax.all_gather(scale_down, 'fs', axis=0, tiled=True)  104 us
    reduce_scatter x2, waiting for transfers between devices, per_device(): lax.psum_scatter((product * piece_scale[:, None]).astype(jnp.bfloat16), '...  44.6 us
    ppermute x3, starting transfers between devices, create_widths(): z[h] = lax.ppermute(z[h + 1], perm=arrivals, axis_name=axis_key)  36 us
    all_gather x1, waiting for transfers between devices, per_device(): lax.all_gather(tokens, 'tp', axis=1, tiled=True).astype(jnp.float32)  35.4 us
    all_gather x1, waiting for transfers between devices, per_device(): lax.all_gather(weight_u.astype(jnp.bfloat16), 'fs', axis=0, tiled=True)  28.8 us
    dot_general x1, matrix products, per_device(): lax.dot_general(columns, hidden, (((0,), (1,)), ((), ())), preferred_elem...  25.7 us
    all_gather x1, waiting for transfers between devices, per_device(): full_out = lax.all_gather(out_rounded, 'fs', axis=1, tiled=True)  17.9 us
  transfers between devices with their start and end apart: 11, of which 8 were waited for; matrix products, arithmetic and copies ran while one was open for 6% of the time, Pallas kernels for 0%

profile of v1, /device:TPU:0, one launch (start us, length us, event | category | flops | bytes accessed | tf_op | source)
XLA Modules:
  0.0 539.6 jit_solution(9207090641243520211)
XLA Ops:
  6.5 1.8 convert_element_type.71
  9.2 1.8 convert_element_type.76
  11.0 1.8 convert_element_type.70
  12.9 1.5 fusion.8
  14.4 14.0 %all-gather = f32[4,1,512]{2,1,0:T(1,128)S(1)} all-gather(f32[1,1,512]{2,1,0:T(1,128)} %bitcast.30), channel_id=1, replica_groups=mesh['grp'=2,'fs'=4,'tp'=4] {'fs'}, dimensions={0}, use_global_device_ids=true | all-gather | bytes 10240 | tf_op jit(solution)/shard_map/all_gather | solution.py:43
  28.4 6.0 %psum.28 = f32[1024]{0:T(1024)S(1)} all-reduce(f32[1024]{0:T(1024)S(1)} %fusion.8), channel_id=1, replica_groups=mesh['grp'=2,'fs'=4,'tp'=4] {'tp'}, use_global_device_ids=true, to_apply=%region_1.0 | all-reduce | flops 1024 | bytes 8192 | tf_op jit(solution)/shard_map/psum | solution.py:51
  34.5 5.2 all-gather.13.cloned.1.call-done
  39.7 35.4 %all-gather.9.cloned.1.call-done = bf16[1024,2048]{1,0:T(8,128)(2,1)} async-done(((bf16[1024,512]{1,0:T(8,128)(2,1)}), bf16[1024,2048]{1,0:T(8,128)(2,1)}) %all-gather.9.cloned.1.call-update) | async-done | bytes 4194320 | tf_op jit(solution)/shard_map/all_gather | solution.py:55
  75.2 4.2 fusion.47
  79.3 6.0 %all-reduce = (f32[1024]{0:T(1024)S(1)}, f32[1024]{0:T(1024)S(1)}) all-reduce(f32[1024]{0:T(1024)S(1)} %get-tuple-element.6, f32[1024]{0:T(1024)S(1)} %get-tuple-element.5), channel_id=1, replica_groups=mesh['grp'=2,'fs'=4,'tp'=4] {'tp'}, use_global_device_ids=true, to_apply=%region_5.0 | all-reduce | flops 2048 | bytes 16384 | tf_op jit(solution)/shard_map/psum | solution.py:64
  85.7 1.1 convolution_add_fusion
  86.9 17.9 %all-gather.15.cloned.1.call-done = bf16[256,2048]{1,0:T(8,128)(2,1)} async-done(((bf16[256,512]{1,0:T(8,128)(2,1)}), bf16[256,2048]{1,0:T(8,128)(2,1)}) %all-gather.15.cloned.1.call-update) | async-done | bytes 1048592 | tf_op jit(solution)/shard_map/all_gather | solution.py:81
  104.7 28.8 %all-gather.11.cloned.1.call-done = bf16[2048,256]{1,0:T(8,128)(2,1)} async-done(((bf16[512,256]{1,0:T(8,128)(2,1)}), bf16[2048,256]{1,0:T(8,128)(2,1)}) %all-gather.11.cloned.1.call-update) | async-done | bytes 1048592 | tf_op jit(solution)/shard_map/all_gather | solution.py:47
  133.6 9.3 %fusion.7 = bf16[2048,1024]{0,1:T(8,128)(2,1)} fusion(f32[2048]{0:T(1024)S(1)} %bitcast.28, bf16[256,2048]{1,0:T(8,128)(2,1)} %all-gather.15.cloned.1.call-done, f32[1024,256]{1,0:T(8,128)S(1)} %bitcast.27, bf16[2048,256]{1,0:T(8,128)(2,1)} %all-gather.11.cloned.1.call-done, bf16[1024,2048]{1,0:T(8,128)(2,1)} %all-gather.9.cloned.1.call-done, ...), kind=kOutput, calls=%fused_computation.9 | convolution fusion | flops 2162950144 | bytes 11555840 | tf_op jit(solution)/shard_map/dot_general | solution.py:84
  143.0 3.9 convert_element_type.84
  147.0 3.0 convert_element_type.81
  150.1 1.6 collective-permute-start
  151.7 47.0 %collective-permute-done = bf16[2048,512]{1,0:T(8,128)(2,1)S(1)} collective-permute-done((bf16[2048,512]{1,0:T(8,128)(2,1)S(1)}, bf16[2048,512]{1,0:T(8,128)(2,1)S(1)}, u32[]{:S(2)}, u32[]{:S(2)}) %collective-permute-start) | collective-permute-done | bytes 2097184 | tf_op jit(solution)/shard_map/ppermute | solution.py:17
  198.7 2.7 fusion.10
  201.4 91.2 %collective-permute-done.1 = bf16[2048,512]{1,0:T(8,128)(2,1)} collective-permute-done((bf16[2048,512]{1,0:T(8,128)(2,1)S(1)}, bf16[2048,512]{1,0:T(8,128)(2,1)}, u32[]{:S(2)}, u32[]{:S(2)}) %collective-permute-start.1) | collective-permute-done | bytes 2097184 | tf_op jit(solution)/shard_map/ppermute | solution.py:17
  292.6 34.4 %collective-permute-start.2 = (bf16[2048,512]{1,0:T(8,128)(2,1)}, bf16[2048,512]{1,0:T(8,128)(2,1)}, u32[]{:S(2)}, u32[]{:S(2)}) collective-permute-start(bf16[2048,512]{1,0:T(8,128)(2,1)} %collective-permute-done.1), channel_id=1, source_target_pairs={{0,4},{4,8},{8,12},{12,0},{1,5},{5,9},{9,13},{13,1},{2,6},{6,10},{... | collective-permute-start | bytes 6291464 | tf_op jit(solution)/shard_map/ppermute | solution.py:17
  327.0 103.9 %all-gather.1 = f32[4,1,512]{2,1,0:T(1,128)S(1)} all-gather(f32[1,1,512]{2,1,0:T(1,128)S(1)} %bitcast.31), channel_id=1, replica_groups=mesh['grp'=2,'fs'=4,'tp'=4] {'fs'}, dimensions={0}, use_global_device_ids=true | all-gather | bytes 10240 | tf_op jit(solution)/shard_map/all_gather | solution.py:44
  430.9 2.1 constant_dynamic-update-slice_fusion.7
  433.1 2.2 constant_dynamic-update-slice_fusion.6
  435.9 1.9 constant_dynamic-update-slice_fusion.3
  437.9 1.9 constant_dynamic-update-slice_fusion.2
  440.5 5.7 %copy-done.5 = bf16[2048,4096]{1,0:T(8,128)(2,1)} copy-done((bf16[2048,4096]{1,0:T(8,128)(2,1)}, bf16[2048,4096]{1,0:T(8,128)(2,1)S(1)}, u32[]{:S(2)}) %copy-start.5) | copy-done | bytes 16777240
  446.2 6.5 %psum.31 = f32[1024]{0:T(1024)S(1)} all-reduce(f32[1024]{0:T(1024)S(1)} %get-tuple-element.9), channel_id=1, replica_groups=mesh['grp'=2,'fs'=4,'tp'=4] {'tp'}, use_global_device_ids=true, to_apply=%region_8.9 | all-reduce | flops 1024 | bytes 8192 | tf_op jit(solution)/shard_map/psum | solution.py:100
  452.7 7.2 %all-gather.17.cloned.1.call-done = bf16[1024,2048]{1,0:T(8,128)(2,1)} async-done(((bf16[1024,512]{1,0:T(8,128)(2,1)}), bf16[1024,2048]{1,0:T(8,128)(2,1)}) %all-gather.17.cloned.1.call-update) | async-done | bytes 4194320 | tf_op jit(solution)/shard_map/all_gather | solution.py:104
  459.9 25.7 %multiply_convert_fusion = bf16[2048,1024]{0,1:T(8,128)(2,1)} fusion(f32[2048]{0:T(1024)S(1)} %bitcast.29, bf16[2048,4096]{1,0:T(8,128)(2,1)} %copy-done.5, s32[]{:T(128)S(6)} %select_n.38, bf16[2048,2048]{1,0:T(8,128)(2,1)} %all-gather.19.cloned.1.call-done, bf16[1024,2048]{1,0:T(8,128)(2,1)} %all-gather.17.cloned.1.call-done, f32[2048]{0:T(1024)S(1)} %copy-done.9, ...), kind=kOutput, calls=%fused_computation | convolution fusion | flops 17200840704 | bytes 25194500 | tf_op jit(solution)/shard_map/dot_general | solution.py:114
  485.7 44.6 %reduce-scatter.5.cloned.1.call-done = bf16[512,1024]{0,1:T(8,128)(2,1)} async-done(((bf16[2048,1024]{0,1:T(8,128)(2,1)}), bf16[512,1024]{0,1:T(8,128)(2,1)}) %reduce-scatter.5.cloned.1.call-update) | async-done | bytes 1048592 | tf_op jit(solution)/shard_map/reduce_scatter | solution.py:118
  530.3 2.5 fusion.11
  (52 shorter events, 2.9 us)
Async XLA Ops:
  6.5 27.9 %copy-start = (f32[4,128]{1,0:T(4,128)S(1)}, f32[4,128]{1,0:T(4,128)}, u32[]{:S(2)}) copy-start(f32[4,128]{1,0:T(4,128)} %param.24) | copy-start | bytes 6148
  6.5 33.2 %all-gather.13.cloned.1.call-start = ((), (), s32[]{:S(2)}) async-start(), calls=%async_computation.4 | async-start | bytes 1310720 | tf_op jit(solution)/shard_map/all_gather | solution.py:48
  8.4 66.8 %all-gather.9.cloned.1.call-start = ((), (), s32[]{:S(2)}) async-start(), calls=%async_computation.2 | async-start | bytes 5242880 | tf_op jit(solution)/shard_map/all_gather | solution.py:55
  9.1 95.6 %all-gather.15.cloned.1.call-start = ((), (), s32[]{:S(2)}) async-start(), calls=%async_computation.5 | async-start | bytes 1310720 | tf_op jit(solution)/shard_map/all_gather | solution.py:81
  11.0 122.6 %all-gather.11.cloned.1.call-start = ((), (), s32[]{:S(2)}) async-start(), calls=%async_computation.3 | async-start | bytes 1310720 | tf_op jit(solution)/shard_map/all_gather | solution.py:47
  12.8 185.9 %reduce-scatter.3.cloned.1.call-start = ((), (), s32[]{:S(2)}) async-start(), calls=%async_computation.6 | async-start | bytes 5242880 | tf_op jit(solution)/shard_map/reduce_scatter | solution.py:88
  34.5 50.9 %copy-start.7 = (f32[256]{0:T(256)S(1)}, f32[256]{0:T(256)}, u32[]{:S(2)}) copy-start(f32[256]{0:T(256)} %param.22) | copy-start | bytes 3076
  34.5 99.1 %copy-start.8 = (f32[2048]{0:T(1024)S(1)}, f32[2048]{0:T(1024)}, u32[]{:S(2)}) copy-start(f32[2048]{0:T(1024)} %param.17) | copy-start | bytes 24580
  34.5 99.1 %copy-start.11 = (f32[256]{0:T(256)S(1)}, f32[256]{0:T(256)}, u32[]{:S(2)}) copy-start(f32[256]{0:T(256)} %param.20) | copy-start | bytes 3076
  142.9 55.8 %copy-start.4 = (bf16[1024,512]{1,0:T(8,128)(2,1)S(1)}, bf16[1024,512]{1,0:T(8,128)(2,1)}, u32[]{:S(2)}) copy-start(bf16[1024,512]{1,0:T(8,128)(2,1)} %param.16) | copy-start | bytes 3145732
  142.9 184.1 %copy-start.6 = (f32[512]{0:T(512)S(1)}, f32[512]{0:T(512)}, u32[]{:S(2)}) copy-start(f32[512]{0:T(512)} %param.31) | copy-start | bytes 6148
  143.0 309.7 %all-gather.19.cloned.1.call-start = ((), (), s32[]{:S(2)}) async-start(), calls=%async_computation.8 | async-start | bytes 10485760 | tf_op jit(solution)/shard_map/all_gather | solution.py:98
  147.0 313.0 %all-gather.17.cloned.1.call-start = ((), (), s32[]{:S(2)}) async-start(), calls=%async_computation.7 | async-start | bytes 5242880 | tf_op jit(solution)/shard_map/all_gather | solution.py:104
  150.1 48.6 %collective-permute-start = (bf16[2048,512]{1,0:T(8,128)(2,1)S(1)}, bf16[2048,512]{1,0:T(8,128)(2,1)S(1)}, u32[]{:S(2)}, u32[]{:S(2)}) collective-permute-start(bf16[2048,512]{1,0:T(8,128)(2,1)S(1)} %convert_element_type.81), channel_id=1, source_target_pairs={{0,4},{4,8},{8,12},{12,0},{1,5},{5,9},{9,13},{13,1},{2,6},{6,10},{... | collective-permute-start | bytes 6291464 | tf_op jit(solution)/shard_map/ppermute | solution.py:17
  198.7 93.9 %collective-permute-start.1 = (bf16[2048,512]{1,0:T(8,128)(2,1)S(1)}, bf16[2048,512]{1,0:T(8,128)(2,1)}, u32[]{:S(2)}, u32[]{:S(2)}) collective-permute-start(bf16[2048,512]{1,0:T(8,128)(2,1)S(1)} %collective-permute-done), channel_id=1, source_target_pairs={{0,4},{4,8},{8,12},{12,0},{1,5},{5,9},{9,13},{13,1},{2,6},{6,10},{... | collective-permute-start | bytes 6291464 | tf_op jit(solution)/shard_map/ppermute | solution.py:17
  201.4 328.9 %reduce-scatter.5.cloned.1.call-start = ((), (), s32[]{:S(2)}) async-start(), calls=%async_computation.9 | async-start | bytes 5242880 | tf_op jit(solution)/shard_map/reduce_scatter | solution.py:118
  292.6 138.3 %collective-permute-start.2 = (bf16[2048,512]{1,0:T(8,128)(2,1)}, bf16[2048,512]{1,0:T(8,128)(2,1)}, u32[]{:S(2)}, u32[]{:S(2)}) collective-permute-start(bf16[2048,512]{1,0:T(8,128)(2,1)} %collective-permute-done.1), channel_id=1, source_target_pairs={{0,4},{4,8},{8,12},{12,0},{1,5},{5,9},{9,13},{13,1},{2,6},{6,10},{... | collective-permute-start | bytes 6291464 | tf_op jit(solution)/shard_map/ppermute | solution.py:17
  327.0 108.6 %copy-start.2 = (f32[2048,512]{1,0:T(8,128)S(1)}, f32[2048,512]{1,0:T(8,128)}, u32[]{:S(2)}) copy-start(f32[2048,512]{1,0:T(8,128)} %param.30) | copy-start | bytes 12582916
  437.8 22.1 %copy-start.9 = (f32[2048]{0:T(1024)S(1)}, f32[2048]{0:T(1024)}, u32[]{:S(2)}) copy-start(f32[2048]{0:T(1024)} %param.29) | copy-start | bytes 24580
  437.9 22.1 %copy-start.10 = (f32[2048]{0:T(1024)S(1)}, f32[2048]{0:T(1024)}, u32[]{:S(2)}) copy-start(f32[2048]{0:T(1024)} %param.27) | copy-start | bytes 24580
  440.5 5.7 %copy-start.5 = (bf16[2048,4096]{1,0:T(8,128)(2,1)}, bf16[2048,4096]{1,0:T(8,128)(2,1)S(1)}, u32[]{:S(2)}) copy-start(bf16[2048,4096]{1,0:T(8,128)(2,1)S(1)} %constant_dynamic-update-slice_fusion) | copy-start | bytes 50331652
  459.9 70.3 %copy-start.3 = (bf16[1024,512]{1,0:T(8,128)(2,1)S(1)}, bf16[1024,512]{1,0:T(8,128)(2,1)}, u32[]{:S(2)}) copy-start(bf16[1024,512]{1,0:T(8,128)(2,1)} %get-tuple-element.10) | copy-start | bytes 3145732
  459.9 72.9 %copy-start.1 = (f32[4,128]{1,0:T(4,128)S(1)}, f32[4,128]{1,0:T(4,128)}, u32[]{:S(2)}) copy-start(f32[4,128]{1,0:T(4,128)} %param.24) | copy-start | bytes 6148
Sparse Core Ops, SparseCore 0:
  8.9 30.7 all-gather.12
  41.3 33.8 all-gather.8
  76.7 27.9 all-gather.14
  106.2 27.3 all-gather.10
  143.0 43.7 reduce-scatter.2
  188.3 238.4 all-gather.18
  428.3 31.5 all-gather.16
  485.8 44.3 reduce-scatter.4
